TPU v7x, 32 devices: a whole 2x2x4 slice. The times are simulated.
32 devices in a mesh: sp: 8 (over z, y), tp: 4 (over x, core).
Axes of the slice: x: 2, y: 2, z: 4, core: 2. Of those that a mesh axis runs over, the one named last changes fastest.
Arguments:
- tokens: bfloat16 [1536, 2048], P('sp'), may hold values from -10 to 10
- w_query: bfloat16 [2048, 1024], P(None, 'tp'), may hold values from -0.125 to 0.125
- w_key: bfloat16 [2048, 256], P(None, 'tp'), may hold values from -0.125 to 0.125
- w_value: bfloat16 [2048, 256], P(None, 'tp'), may hold values from -0.125 to 0.125
- w_output: bfloat16 [1024, 2048], P('tp'), may hold values from -0.1875 to 0.1875
- query_gain: float32 [64], replicated, may hold values from 0.4 to 9
- key_gain: float32 [64], replicated, may hold values from 0.4 to 9
Outputs:
- mixed_out: bfloat16 [1536, 2048], P(('sp', 'tp'))
- log_sums: float32 [16, 1536], P('tp', 'sp')
All inputs are finite; a program needn't handle non-finite values.
Results may differ from a plain program's by a relative error of at most 0.009.
The roundings to bfloat16 on the way count: a program that leaves them out, or rounds other values in their place, can miss the bound.
Values may be sent and summed in bfloat16 or wider, within the bound.
A program may use at most 64 MiB of HBM per device.

v0:
```python
import math

import jax
import jax.numpy as jnp
from jax import lax
from jax.sharding import PartitionSpec as P

GRID_W = 64


ROPE_BASE = 10000.0
NORM_EPS = 1e-06


def rotate(values, position):
    dim = values.shape[-1]
    half_dim = dim // 2
    inverse = ROPE_BASE ** (-jnp.arange(half_dim, dtype=jnp.float32) * (2.0 / dim))
    angles = position.astype(jnp.float32)[:, None] * inverse[None, :]
    cosine = jnp.cos(angles)[:, None, :]
    sine = jnp.sin(angles)[:, None, :]
    first_half = values[..., :half_dim]
    second_half = values[..., half_dim:]
    return jnp.concatenate(
        [first_half * cosine - second_half * sine, second_half * cosine + first_half * sine], -1
    )


def prepare(projected, gain_vec, grid_row, grid_col):
    values = projected.astype(jnp.float32)
    values = values * lax.rsqrt(jnp.mean(values * values, -1, keepdims=True) + NORM_EPS) * gain_vec
    split_at = values.shape[-1] // 2
    turned = jnp.concatenate(
        [rotate(values[..., :split_at], grid_row), rotate(values[..., split_at:], grid_col)], -1
    )
    return turned.astype(jnp.bfloat16)


def shards(tokens, w_query, w_key, w_value, w_output, query_gain, key_gain):
    head_dim = query_gain.shape[0]
    n_query = w_query.shape[1]
    n_key = w_key.shape[1]
    combined = jnp.concatenate([w_query, w_key, w_value], axis=1)
    projected = jnp.dot(tokens, combined, preferred_element_type=jnp.float32).astype(jnp.bfloat16)
    seq_rows = projected.shape[0]
    local_heads = n_query // head_dim
    local_kv = n_key // head_dim
    group_size = local_heads // local_kv
    positions = lax.axis_index("sp") * seq_rows + jnp.arange(seq_rows, dtype=jnp.int32)
    grid_row = positions // GRID_W
    grid_col = positions % GRID_W
    queries = prepare(
        projected[:, :n_query].reshape(seq_rows, local_heads, head_dim),
        query_gain,
        grid_row,
        grid_col,
    )
    key_rows = prepare(
        projected[:, n_query : n_query + n_key].reshape(seq_rows, local_kv, head_dim),
        key_gain,
        grid_row,
        grid_col,
    )
    key_value = jnp.concatenate(
        [key_rows.reshape(seq_rows, n_key), projected[:, n_query + n_key :]], axis=1
    )
    grouped = queries.reshape(seq_rows, local_kv, group_size, head_dim).transpose(1, 2, 0, 3)
    grouped = grouped.reshape(local_kv, group_size * seq_rows, head_dim)
    score_scale = head_dim ** (-0.5)
    initial = (
        jnp.full((local_kv, group_size * seq_rows), -1e30, jnp.float32),
        jnp.zeros((local_kv, group_size * seq_rows), jnp.float32),
        jnp.zeros((local_kv, group_size * seq_rows, head_dim), jnp.float32),
    )
    gathered = lax.all_gather(key_value, "sp", axis=0, tiled=True)
    piece_rows = gathered.shape[0]
    span_rows = math.gcd(piece_rows, 1024)
    pieces = gathered.reshape(piece_rows // span_rows, span_rows, 2, local_kv, head_dim)

    def update(state, block):
        running, totals, weighted = state
        key_block = block[:, 0]
        value_block = block[:, 1]
        scores = (
            jnp.einsum("kqd,skd->kqs", grouped, key_block, preferred_element_type=jnp.float32)
            * score_scale
        )
        new_max = jnp.maximum(running, jnp.max(scores, -1))
        shrink = jnp.exp(running - new_max)
        expos = jnp.exp(scores - new_max[..., None])
        totals = totals * shrink + jnp.sum(expos, -1)
        weighted = weighted * shrink[..., None] + jnp.einsum(
            "kqs,skd->kqd",
            expos.astype(jnp.bfloat16),
            value_block,
            preferred_element_type=jnp.float32,
        )
        return ((new_max, totals, weighted), None)

    result, unused = lax.scan(update, initial, pieces)
    running, totals, weighted = result
    attended = (weighted / totals[..., None]).astype(jnp.bfloat16)
    attended = (
        attended.reshape(local_kv, group_size, seq_rows, head_dim)
        .transpose(2, 0, 1, 3)
        .reshape(seq_rows, n_query)
    )
    log_sums = (running + jnp.log(totals)).reshape(local_heads, seq_rows)
    mixed_out = lax.psum_scatter(
        jnp.dot(attended, w_output, preferred_element_type=jnp.float32),
        "tp",
        scatter_dimension=0,
        tiled=True,
    ).astype(jnp.bfloat16)
    return (mixed_out, log_sums)


def solution(mesh):
    placed = (P("sp", None), P(None, "tp"), P(None, "tp"), P(None, "tp"), P("tp", None), P(), P())
    return jax.shard_map(
        shards,
        mesh=mesh,
        in_specs=placed,
        out_specs=(P(("sp", "tp"), None), P("tp", "sp")),
        check_vma=False,
    )
```

profile of v0, /device:TPU:0, one launch (start us, length us, event | category | flops | bytes accessed | tf_op | source)
XLA Modules:
  0.0 90.4 jit_solution(16520962171789180682)
XLA Ops:
  7.3 1.3 %copy.35 = bf16[2048,64]{1,0:T(8,128)(2,1)S(1)} copy(bf16[2048,64]{0,1:T(8,128)(2,1)} %param.12) | data formatting | bytes 524288 | tf_op args[3]
  8.6 1.2 %copy.34 = bf16[2048,64]{1,0:T(8,128)(2,1)S(1)} copy(bf16[2048,64]{0,1:T(8,128)(2,1)} %param.11) | data formatting | bytes 524288 | tf_op args[2]
  9.8 2.3 %fusion.18 = bf16[192,384]{0,1:T(8,128)(2,1)S(1)} fusion(bf16[192,2048]{1,0:T(8,128)(2,1)} %param.9, bf16[2048,64]{1,0:T(8,128)(2,1)S(1)} %copy.35, bf16[2048,64]{1,0:T(8,128)(2,1)S(1)} %copy.34, bf16[2048,256]{1,0:T(8,128)(2,1)} %param.10), kind=kOutput, calls=%fused_computation.26 | convolution fusion | flops 306782208 | bytes 2506752 | tf_op jit(solution)/shard_map/dot_general | solution.py:44
  12.6 0.2 multiply_cosine_fusion.1
  12.8 0.1 constant_dynamic-update-slice_fusion.1
  13.2 32.8 %all_gather.3 = bf16[1536,128]{1,0:T(8,128)(2,1)S(1)} all-gather(bf16[192,128]{1,0:T(8,128)(2,1)S(1)} %copy.37), channel_id=1, replica_groups=mesh['sp'=8,'tp'=4] {'sp'}, dimensions={0}, use_global_device_ids=true | all-gather | bytes 442368 | tf_op jit(solution)/shard_map/all_gather | solution.py:75
  46.0 0.3 reshape.403
  46.4 0.6 copy.40
  47.1 0.2 copy.46
  47.3 3.5 %while.15 = (s32[]{:T(128)}, f32[1,768]{1,0:T(1,128)S(1)}, f32[1,768]{1,0:T(1,128)S(1)}, f32[1,768,64]{1,2,0:T(8,128)S(1)}, bf16[3,512,2,1,64]{1,4,3,2,0:T(8,128...) while((s32[]{:T(128)}, f32[1,768]{1,0:T(1,128)S(1)}, ...), condition=%wide.region_5.6_spmd.clone, body=%wide.region_2.5_spmd.clone.sunk | while | flops 103174656 | bytes 5756013 | solution.py:100
  47.3 0.4 fusion.62
  47.8 0.3 fusion.64
  48.1 0.4 fusion.66
  48.5 0.4 fusion.62
  49.0 0.3 fusion.64
  49.2 0.4 fusion.66
  49.7 0.4 fusion.62
  50.1 0.3 fusion.64
  50.4 0.4 fusion.66
  50.9 0.2 reshape.396
  51.1 1.6 %fusion.51 = f32[192,2048]{1,0:T(8,128)} fusion(bf16[192,256]{0,1:T(8,128)(2,1)S(1)} %bitcast.65, bf16[256,2048]{1,0:T(8,128)(2,1)S(1)} %copy-done), kind=kOutput, calls=%fused_computation.91 | convolution fusion | flops 201326592 | bytes 2719744 | tf_op jit(solution)/shard_map/dot_general | solution.py:110
  52.7 0.7 reshape.398
  53.3 28.5 %reduce-scatter.2.cloned.1.call-done = f32[48,2048]{1,0:T(8,128)} async-done(((f32[192,2048]{1,0:T(8,128)}), f32[48,2048]{1,0:T(8,128)}) %reduce-scatter.2.cloned.1.call-update) | async-done | bytes 393232 | tf_op jit(solution)/shard_map/reduce_scatter | solution.py:109
  81.9 1.7 %convert_element_type.63 = bf16[48,2048]{1,0:T(8,128)(2,1)} convert(f32[48,2048]{1,0:T(8,128)} %reduce-scatter.2.cloned.1.call-done) | non-fusion elementwise | flops 98304 | bytes 589824 | tf_op jit(solution)/shard_map/convert_element_type | solution.py:114
  (41 shorter events, 1.2 us)
Async XLA Ops:
  7.2 43.9 %copy-start = (bf16[256,2048]{1,0:T(8,128)(2,1)S(1)}, bf16[256,2048]{1,0:T(8,128)(2,1)}, u32[]{:S(2)}) copy-start(bf16[256,2048]{1,0:T(8,128)(2,1)} %param.13) | copy-start | bytes 3145732
  7.2 74.7 %reduce-scatter.2.cloned.1.call-start = ((), (), s32[]{:S(2)}) async-start(), calls=%async_computation.1 | async-start | bytes 1966080 | tf_op jit(solution)/shard_map/reduce_scatter | solution.py:109
  9.8 2.4 %copy-start.1 = (f32[64]{0:T(128)S(1)}, f32[64]{0:T(128)}, u32[]{:S(2)}) copy-start(f32[64]{0:T(128)} %param.15) | copy-start | bytes 772
  12.6 34.3 %copy-start.2 = (f32[64]{0:T(128)S(1)}, f32[64]{0:T(128)}, u32[]{:S(2)}) copy-start(f32[64]{0:T(128)} %param.14) | copy-start | bytes 772
Sparse Core Ops, SparseCore 0:
  52.8 29.0 reduce-scatter.1
where the time goes:
time: 90.7 us; the launch traced here: 90.4 us
  blocking collectives  32.8 us (36%)
  waiting for transfers between devices  28.6 us (32%)
  between operations  14.3 us (16%)
  matrix products  6.26 us (7%)
  local copies, waits for them, and re-layouts  4.62 us (5%)
  other arithmetic  3.75 us (4%)
    all_gather x1, blocking collectives, shards(): gathered = lax.all_gather(key_value, 'sp', axis=0, tiled=True)  32.8 us
    reduce_scatter x1, waiting for transfers between devices, shards(): lax.psum_scatter(jnp.dot(attended, w_output, preferred_element_type=jnp.f...  28.5 us
    unnamed x10, local copies, waits for them, and re-layouts  3.26 us
    dot_general x1, matrix products, shards(): jnp.dot(tokens, combined, preferred_element_type=jnp.float32)  2.29 us
  transfers between devices with their start and end apart: 1, of which 1 were waited for; matrix products, arithmetic and copies ran while one was open for 1% of the time, Pallas kernels for 0%

commit v1 on v0

v1 whole, which is shorter than its diff:
```python
import functools
import math

import jax
import jax.numpy as jnp
from jax import lax
from jax.experimental import pallas as pl
from jax.experimental.pallas import tpu as pltpu
from jax.sharding import PartitionSpec as P

GRID_W = 64
ROPE_BASE = 10000.0
NORM_EPS = 1e-06
CHUNKS = 4
MESH = pl.DeviceIdType.MESH
F32 = jnp.float32
BF16 = jnp.bfloat16


def column(row_vec):
    n = row_vec.shape[1]
    down = lax.broadcasted_iota(jnp.int32, (n, n), 0)
    across = lax.broadcasted_iota(jnp.int32, (n, n), 1)
    spread = jnp.where(down == across, jnp.broadcast_to(row_vec, (n, n)), 0.0)
    return jnp.sum(spread, axis=1, keepdims=True)


def tables(first, rows, copies, half):
    shape = (half, copies * rows)
    lane = lax.broadcasted_iota(jnp.int32, shape, 1)
    for c in range(copies - 1, 0, -1):
        lane = jnp.where(lane >= c * rows, lane - c * rows, lane) if c == 1 else jnp.where(
            lane >= c * rows, lane - (c - 1) * rows, lane
        )
    position = lane + first
    index = lax.broadcasted_iota(jnp.int32, shape, 0).astype(F32)
    inverse = jnp.exp(index * (-math.log(ROPE_BASE) / half))
    shift = GRID_W.bit_length() - 1
    row = lax.shift_right_logical(position, shift).astype(F32) * inverse
    col = jnp.bitwise_and(position, GRID_W - 1).astype(F32) * inverse
    return jnp.cos(row), jnp.sin(row), jnp.cos(col), jnp.sin(col)


def prepare(values, gain_col, tabs):
    head = values.shape[0]
    w = head // 4
    values = values * lax.rsqrt(jnp.mean(values * values, 0, keepdims=True) + NORM_EPS) * gain_col
    cr, sr, cc, sc = tabs
    a, b, c, d = (values[i * w : (i + 1) * w] for i in range(4))
    return jnp.concatenate(
        [a * cr - b * sr, b * cr + a * sr, c * cc - d * sc, d * cc + c * sc], axis=0
    )


def kernel(
    n_sp, n_tp,
    tok_hbm, wq_hbm, wk_hbm, wv_hbm, wo_hbm, qg_ref, kg_ref,
    out_ref, lse_ref,
    tok, wq, wk, wv, wo, kv_own, kvbuf, qpad, att, send_a, recv_a, keep, send_b, recv_b,
    load_sem, send_sem, fwd_sem, recv_sem, a_send, a_recv, b_send, b_recv,
):
    rows = tok.shape[0]
    head = wk.shape[1]
    heads = wq.shape[1] // head
    lanes = heads * rows
    width = wo.shape[1]
    chunk = width // CHUNKS
    part = rows // n_tp
    n_out = n_sp // 2

    me = lax.axis_index("sp")
    t = lax.axis_index("tp")
    outer = me // 2
    minor = me % 2
    partner = outer * 2 + 1 - minor
    tp_near = t + 1 - 2 * (t % 2)
    tp_far = (t + 2) % 4

    def peer(d):
        return ((outer + d) % n_out) * 2 + minor

    def origin(d):
        return (outer + n_out - d) % n_out

    loads = [
        pltpu.make_async_copy(src, dst, load_sem.at[i])
        for i, (src, dst) in enumerate(
            [(tok_hbm, tok), (wk_hbm, wk), (wv_hbm, wv), (wq_hbm, wq), (wo_hbm, wo)]
        )
    ]
    for load in loads[:4]:
        load.start()

    barrier = pltpu.get_barrier_semaphore()
    pl.semaphore_signal(barrier, inc=1, device_id={"sp": partner}, device_id_type=MESH)
    pl.semaphore_signal(barrier, inc=1, device_id={"tp": tp_near}, device_id_type=MESH)
    pl.semaphore_signal(barrier, inc=1, device_id={"tp": tp_far}, device_id_type=MESH)

    def greet(d, unused):
        pl.semaphore_signal(barrier, inc=1, device_id={"sp": peer(d)}, device_id_type=MESH)
        return unused

    lax.fori_loop(1, n_out, greet, 0)

    tabs = tables(me * rows, rows, heads, head // 4)
    key_tabs = tuple(x[:, :rows] for x in tabs)
    gain_q = column(qg_ref[...]) * (head ** -0.5)
    gain_k = column(kg_ref[...])

    loads[0].wait()
    loads[1].wait()
    loads[2].wait()
    loads[4].start()
    w_kv = jnp.concatenate([wv[...], wk[...]], axis=1)
    raw = jnp.dot(tok[...], w_kv, preferred_element_type=F32).astype(BF16).astype(F32)
    raw_t = raw.T
    keys_t = prepare(raw_t[head:], gain_k, key_tabs)
    kv_own[...] = jnp.concatenate([raw_t[:head], keys_t], axis=0).T.astype(BF16)

    def slot(i):
        return kvbuf.at[pl.ds(pl.multiple_of(i * rows, 16), rows), :]

    def to_partner():
        return pltpu.make_async_remote_copy(
            src_ref=kv_own, dst_ref=slot(me), send_sem=send_sem.at[0], recv_sem=recv_sem.at[me],
            device_id={"sp": partner}, device_id_type=MESH,
        )

    def to_peer(d):
        return pltpu.make_async_remote_copy(
            src_ref=kv_own, dst_ref=slot(me), send_sem=send_sem.at[d], recv_sem=recv_sem.at[me],
            device_id={"sp": peer(d)}, device_id_type=MESH,
        )

    def forward(d):
        i = origin(d) * 2 + minor
        return pltpu.make_async_remote_copy(
            src_ref=slot(i), dst_ref=slot(i), send_sem=fwd_sem.at[d], recv_sem=recv_sem.at[i],
            device_id={"sp": partner}, device_id_type=MESH,
        )

    def arrival(i):
        pltpu.make_async_remote_copy(
            src_ref=slot(i), dst_ref=slot(i), send_sem=send_sem.at[0], recv_sem=recv_sem.at[i],
            device_id={"sp": partner}, device_id_type=MESH,
        ).wait_recv()
        return kvbuf[pl.ds(pl.multiple_of(i * rows, 16), rows), :]

    pl.semaphore_wait(barrier, n_out + 2)

    def send_peer(d, unused):
        to_peer(d).start()
        return unused

    lax.fori_loop(1, n_out, send_peer, 0)
    to_partner().start()

    loads[3].wait()
    raw_q = jnp.dot(tok[...], wq[...], preferred_element_type=F32).astype(BF16).astype(F32)
    stacked = jnp.concatenate([raw_q[:, h * head : (h + 1) * head] for h in range(heads)], axis=0)
    queries = prepare(stacked.T, gain_q, tabs)
    qpad[...] = jnp.concatenate([jnp.zeros_like(queries), queries], axis=0).astype(BF16)

    def attend(kv, state):
        scores = jnp.dot(kv, qpad[...], preferred_element_type=F32)
        top = jnp.max(scores, axis=0, keepdims=True)
        if state is not None:
            top = jnp.maximum(top, state[0])
        expos = jnp.exp(scores - top)
        total = jnp.sum(expos, axis=0, keepdims=True)
        summed = lax.dot_general(
            kv[:, :head], expos.astype(BF16), (((0,), (0,)), ((), ())), preferred_element_type=F32
        )
        if state is not None:
            shrink = jnp.exp(state[0] - top)
            total = total + state[1] * shrink
            summed = summed + state[2] * shrink
        return top, total, summed

    state = attend(kv_own[...], None)
    state = attend(arrival(partner), state)

    def take_direct(d, state):
        i = origin(d) * 2 + minor
        block = arrival(i)
        forward(d).start()
        return attend(block, state)

    def take_forwarded(d, state):
        return attend(arrival(origin(d) * 2 + 1 - minor), state)

    if n_out <= 8:
        for d in range(1, n_out):
            state = take_direct(d, state)
        for d in range(1, n_out):
            state = take_forwarded(d, state)
    else:
        state = lax.fori_loop(1, n_out, take_direct, state)
        state = lax.fori_loop(1, n_out, take_forwarded, state)
    top, total, summed = state

    result = (summed / total).T.astype(BF16)
    att[...] = jnp.concatenate([result[h * rows : (h + 1) * rows] for h in range(heads)], axis=1)

    def rows_of(j):
        return att[pl.ds(pl.multiple_of(j * part, 16), part), :]

    side, side_minor = t // 2, t % 2
    give = jnp.concatenate(
        [rows_of((1 - side) * 2 + 1 - side_minor), rows_of(side * 2 + 1 - side_minor)], axis=0
    )
    hold = jnp.concatenate([rows_of((1 - side) * 2 + side_minor), rows_of(t)], axis=0)

    loads[4].wait()

    def copy_a(c):
        return pltpu.make_async_remote_copy(
            src_ref=send_a.at[c], dst_ref=recv_a.at[c], send_sem=a_send.at[c], recv_sem=a_recv.at[c],
            device_id={"tp": tp_near}, device_id_type=MESH,
        )

    def copy_b(c):
        return pltpu.make_async_remote_copy(
            src_ref=send_b.at[c], dst_ref=recv_b.at[c], send_sem=b_send.at[c], recv_sem=b_recv.at[c],
            device_id={"tp": tp_far}, device_id_type=MESH,
        )

    for c in range(CHUNKS):
        cols = slice(c * chunk, (c + 1) * chunk)
        send_a[c] = jnp.dot(give, wo[:, cols], preferred_element_type=F32).astype(BF16)
        copy_a(c).start()
    for c in range(CHUNKS):
        cols = slice(c * chunk, (c + 1) * chunk)
        mine = jnp.dot(hold, wo[:, cols], preferred_element_type=F32)
        copy_a(c).wait_recv()
        mine = mine + recv_a[c].astype(F32)
        send_b[c] = mine[:part].astype(BF16)
        copy_b(c).start()
        keep[c] = mine[part:]

    logs = top + jnp.log(total)
    for h in range(heads):
        lse_ref[h : h + 1, :] = logs[:, h * rows : (h + 1) * rows]

    for c in range(CHUNKS):
        cols = slice(c * chunk, (c + 1) * chunk)
        copy_b(c).wait_recv()
        out_ref[:, cols] = (keep[c] + recv_b[c].astype(F32)).astype(BF16)

    def drain(d, unused):
        to_peer(d).wait_send()
        forward(d).wait_send()
        return unused

    lax.fori_loop(1, n_out, drain, 0)
    to_partner().wait_send()
    for c in range(CHUNKS):
        copy_a(c).wait_send()
        copy_b(c).wait_send()


def solution(mesh):
    n_sp, n_tp = mesh.shape["sp"], mesh.shape["tp"]

    def shards(tokens, w_query, w_key, w_value, w_output, query_gain, key_gain):
        rows, depth = tokens.shape
        n_query, n_key = w_query.shape[1], w_key.shape[1]
        head = query_gain.shape[0]
        heads = n_query // head
        width = w_output.shape[1]
        part = rows // n_tp
        chunk = width // CHUNKS
        n_out = n_sp // 2
        hbm = pl.BlockSpec(memory_space=pl.ANY)
        vmem = pl.BlockSpec(memory_space=pltpu.VMEM)
        dma = pltpu.SemaphoreType.DMA
        return pl.pallas_call(
            functools.partial(kernel, n_sp, n_tp),
            out_shape=(
                jax.ShapeDtypeStruct((part, width), BF16),
                jax.ShapeDtypeStruct((heads, rows), F32),
            ),
            in_specs=[hbm] * 5 + [vmem] * 2,
            out_specs=(vmem, vmem),
            scratch_shapes=[
                pltpu.VMEM((rows, depth), BF16),
                pltpu.VMEM((depth, n_query), BF16),
                pltpu.VMEM((depth, n_key), BF16),
                pltpu.VMEM((depth, n_key), BF16),
                pltpu.VMEM((n_query, width), BF16),
                pltpu.VMEM((rows, 2 * head), BF16),
                pltpu.VMEM((n_sp * rows, 2 * head), BF16),
                pltpu.VMEM((2 * head, heads * rows), BF16),
                pltpu.VMEM((rows, n_query), BF16),
                pltpu.VMEM((CHUNKS, 2 * part, chunk), BF16),
                pltpu.VMEM((CHUNKS, 2 * part, chunk), BF16),
                pltpu.VMEM((CHUNKS, part, chunk), F32),
                pltpu.VMEM((CHUNKS, part, chunk), BF16),
                pltpu.VMEM((CHUNKS, part, chunk), BF16),
                dma((5,)),
                dma((n_out,)),
                dma((n_out,)),
                dma((n_sp,)),
                dma((CHUNKS,)),
                dma((CHUNKS,)),
                dma((CHUNKS,)),
                dma((CHUNKS,)),
            ],
            compiler_params=pltpu.CompilerParams(collective_id=0, has_side_effects=True),
            name="layer",
        )(tokens, w_query, w_key, w_value, w_output, query_gain[None, :], key_gain[None, :])

    placed = (P("sp", None), P(None, "tp"), P(None, "tp"), P(None, "tp"), P("tp", None), P(), P())
    return jax.shard_map(
        shards,
        mesh=mesh,
        in_specs=placed,
        out_specs=(P(("sp", "tp"), None), P("tp", "sp")),
        check_vma=False,
    )
```

time: 90.7 us -> 31.5 us (0.35)
  blocking collectives: 32.8 us -> 0 us
  waiting for transfers between devices: 28.6 us -> 0 us
  Pallas kernels: 0 us -> 25.4 us
  between operations: 14.3 us -> 0.66 us
  matrix products: 6.26 us -> 0 us
  other arithmetic: 3.75 us -> 0 us
    all_gather x1 -> x0, blocking collectives: 32.8 us -> none  [shards(): gathered = lax.all_gather(key_value, 'sp', axis=0, tiled=True)]
    reduce_scatter x1 -> x0, waiting for transfers between devices: 28.5 us -> none  [shards(): lax.psum_scatter(jnp.dot(attended, w_output, preferred_element_type=jnp.f...]
    pallas_call x0 -> x1, Pallas kernels: none -> 25.4 us  [shards(): pl.pallas_call(functools.partial(kernel, n_sp, n_tp), out_shape=(jax.Shap...]
    dot_general x8 -> x0, matrix products: 6.26 us -> none  [the longest x1 2.29 us: shards(): jnp.dot(tokens, combined, preferred_element_type=jnp.float32)]
    unnamed x10 -> x8, local copies, waits for them, and re-layouts: 3.26 us -> 5.22 us
    convert_element_type x3 -> x0, other arithmetic: 1.73 us -> none  [the longest x1 1.69 us: shards(): mixed_out = lax.psum_scatter(jnp.dot(attended, w_output, preferred_elemen...]
    reshape x4 -> x0, local copies, waits for them, and re-layouts: 1.19 us -> none  [the longest x1 0.67 us: shards(): log_sums = (running + jnp.log(totals)).reshape(local_heads, seq_rows)]
  transfers between devices with their start and end apart: 1 -> 0, of which waited for: 1 -> 0; matrix products, arithmetic and copies ran while one was open for 1% -> 0% of each run, Pallas kernels for 0% -> 0%
where the time goes in v1:
time: 31.5 us; the launch traced here: 31.3 us
  Pallas kernels  25.4 us (81%)
  local copies, waits for them, and re-layouts  5.22 us (17%)
  between operations  0.66 us (2%)
    pallas_call x1, Pallas kernels, shards(): pl.pallas_call(functools.partial(kernel, n_sp, n_tp), out_shape=(jax.Shap...  25.4 us
    unnamed x8, local copies, waits for them, and re-layouts  5.22 us

profile of v1, /device:TPU:0, one launch (start us, length us, event | category | flops | bytes accessed | tf_op | source)
XLA Modules:
  0.0 31.3 jit_solution(16022857224728558788)
XLA Ops:
  0.6 0.0 copy-start
  0.6 2.0 %copy.9.wk_hbm = bf16[2048,64]{1,0:T(8,128)(2,1)} copy(bf16[2048,64]{0,1:T(8,128)(2,1)} %param.9) | data formatting | bytes 524288 | tf_op args[2]
  2.6 0.0 copy-done
  2.6 1.0 %copy.10.wv_hbm = bf16[2048,64]{1,0:T(8,128)(2,1)} copy(bf16[2048,64]{0,1:T(8,128)(2,1)S(1)} %copy-done) | data formatting | bytes 524288 | tf_op args[3]
  3.6 25.4 %layer.1 = (bf16[48,2048]{1,0:T(8,128)(2,1)}, f32[4,192]{1,0:T(4,128)}) custom-call(bf16[192,2048]{1,0:T(8,128)(2,1)} %tok_hbm.1, bf16[2048,256]{1,0:T(8,128)(2,1)} %wq_hbm.1, bf16[2048,64]{1,0:T(8,128)(2,1)} %copy.9.wk_hbm, bf16[2048,64]{1,0:T(8,128)(2,1)} %copy.10.wv_hbm, bf16[256,2048]{1,0:T(8,128)(2,1)} %wo_hbm.1, f32[1,64]{1,0:T(1,128)} %bitcast.2, ...), custom_call_target="tpu_custom_call" | custom-call | tf_op jit(solution)/shard_map/layer/pallas_call | solution.py:277
  29.1 0.0 copy-start.1
  29.1 1.6 %copy.13 = bf16[48,2048]{1,0:T(8,128)(2,1)} copy(bf16[48,2048]{1,0:T(8,128)(2,1)} %get-tuple-element.4) | data formatting | bytes 393216
  30.7 0.0 copy-done.1
  30.7 0.6 %copy.14 = f32[4,192]{1,0:T(4,128)} copy(f32[4,192]{1,0:T(4,128)S(1)} %copy-done.1) | data formatting | bytes 6144
Async XLA Ops:
  0.6 2.0 %copy-start = (bf16[2048,64]{0,1:T(8,128)(2,1)S(1)}, bf16[2048,64]{0,1:T(8,128)(2,1)}, u32[]{:S(2)}) copy-start(bf16[2048,64]{0,1:T(8,128)(2,1)} %param.10) | copy-start | bytes 786436
  29.1 1.6 %copy-start.1 = (f32[4,192]{1,0:T(4,128)S(1)}, f32[4,192]{1,0:T(4,128)}, u32[]{:S(2)}) copy-start(f32[4,192]{1,0:T(4,128)} %get-tuple-element.5) | copy-start | bytes 9220

commit v2 on v1

--- a/solution.py
+++ b/solution.py
@@ -56,11 +56,11 @@
     n_sp, n_tp,
     tok_hbm, wq_hbm, wk_hbm, wv_hbm, wo_hbm, qg_ref, kg_ref,
     out_ref, lse_ref,
-    tok, wq, wk, wv, wo, kv_own, kvbuf, qpad, att, send_a, recv_a, keep, send_b, recv_b,
+    tok, wq, w_kv, wo, kv_own, kvbuf, qpad, att, send_a, recv_a, keep, send_b, recv_b,
     load_sem, send_sem, fwd_sem, recv_sem, a_send, a_recv, b_send, b_recv,
 ):
     rows = tok.shape[0]
-    head = wk.shape[1]
+    head = w_kv.shape[0] // 2
     heads = wq.shape[1] // head
     lanes = heads * rows
     width = wo.shape[1]
@@ -85,7 +85,10 @@
     loads = [
         pltpu.make_async_copy(src, dst, load_sem.at[i])
         for i, (src, dst) in enumerate(
-            [(tok_hbm, tok), (wk_hbm, wk), (wv_hbm, wv), (wq_hbm, wq), (wo_hbm, wo)]
+            [
+                (tok_hbm, tok), (wv_hbm, w_kv.at[:head]), (wk_hbm, w_kv.at[head:]),
+                (wq_hbm, wq), (wo_hbm, wo),
+            ]
         )
     ]
     for load in loads[:4]:
@@ -111,9 +114,9 @@
     loads[1].wait()
     loads[2].wait()
     loads[4].start()
-    w_kv = jnp.concatenate([wv[...], wk[...]], axis=1)
-    raw = jnp.dot(tok[...], w_kv, preferred_element_type=F32).astype(BF16).astype(F32)
-    raw_t = raw.T
+    raw_t = lax.dot_general(
+        w_kv[...], tok[...], (((1,), (1,)), ((), ())), preferred_element_type=F32
+    ).astype(BF16).astype(F32)
     keys_t = prepare(raw_t[head:], gain_k, key_tabs)
     kv_own[...] = jnp.concatenate([raw_t[:head], keys_t], axis=0).T.astype(BF16)
 
@@ -271,7 +274,7 @@
         part = rows // n_tp
         chunk = width // CHUNKS
         n_out = n_sp // 2
-        hbm = pl.BlockSpec(memory_space=pl.ANY)
+        hbm = pl.BlockSpec(memory_space=pltpu.HBM)
         vmem = pl.BlockSpec(memory_space=pltpu.VMEM)
         dma = pltpu.SemaphoreType.DMA
         return pl.pallas_call(
@@ -285,8 +288,7 @@
             scratch_shapes=[
                 pltpu.VMEM((rows, depth), BF16),
                 pltpu.VMEM((depth, n_query), BF16),
-                pltpu.VMEM((depth, n_key), BF16),
-                pltpu.VMEM((depth, n_key), BF16),
+                pltpu.VMEM((2 * n_key, depth), BF16),
                 pltpu.VMEM((n_query, width), BF16),
                 pltpu.VMEM((rows, 2 * head), BF16),
                 pltpu.VMEM((n_sp * rows, 2 * head), BF16),
@@ -306,9 +308,9 @@
                 dma((CHUNKS,)),
                 dma((CHUNKS,)),
             ],
-            compiler_params=pltpu.CompilerParams(collective_id=0, has_side_effects=True),
+            compiler_params=pltpu.CompilerParams(collective_id=0, has_side_effects=True, vmem_limit_bytes=24 * 2**20),
             name="layer",
-        )(tokens, w_query, w_key, w_value, w_output, query_gain[None, :], key_gain[None, :])
+        )(tokens, w_query, w_key.T, w_value.T, w_output, query_gain[None, :], key_gain[None, :])
 
     placed = (P("sp", None), P(None, "tp"), P(None, "tp"), P(None, "tp"), P("tp", None), P(), P())
     return jax.shard_map(

time: 31.5 us -> 31.9 us (1.013)
  local copies, waits for them, and re-layouts: 5.22 us -> 7.41 us
  Pallas kernels: 25.4 us -> 23.5 us
    unnamed x8 -> x16, local copies, waits for them, and re-layouts: 5.22 us -> 7.41 us
    pallas_call x1, Pallas kernels: 25.4 us -> 23.5 us  [shards(): pl.pallas_call(functools.partial(kernel, n_sp, n_tp), out_shape=(jax.Shap...]
where the time goes in v2:
time: 31.9 us; the launch traced here: 31.6 us
  Pallas kernels  23.5 us (74%)
  local copies, waits for them, and re-layouts  7.41 us (23%)
  between operations  0.66 us (2%)
    pallas_call x1, Pallas kernels, shards(): pl.pallas_call(functools.partial(kernel, n_sp, n_tp), out_shape=(jax.Shap...  23.5 us
    unnamed x16, local copies, waits for them, and re-layouts  7.41 us

profile of v2, /device:TPU:0, one launch (start us, length us, event | category | flops | bytes accessed | tf_op | source)
XLA Modules:
  0.0 31.6 jit_solution(4120617913453588025)
XLA Ops:
  0.6 0.0 copy-start.5
  0.6 0.0 copy-start.6
  0.7 0.6 %copy-done.5 = f32[64]{0:T(128)S(1)} copy-done((f32[64]{0:T(128)S(1)}, f32[64]{0:T(128)}, u32[]{:S(2)}) %copy-start.5) | copy-done | bytes 280
  1.3 0.0 copy-done.6
  1.3 0.0 copy-start
  1.3 1.2 %copy-done = bf16[2048,256]{1,0:T(8,128)(2,1)S(1)} copy-done((bf16[2048,256]{1,0:T(8,128)(2,1)S(1)}, bf16[2048,256]{1,0:T(8,128)(2,1)}, u32[]{:S(2)}) %copy-start) | copy-done | bytes 1048600
  2.5 0.0 copy-start.1
  2.5 1.2 %copy-done.1 = bf16[256,2048]{1,0:T(8,128)(2,1)S(1)} copy-done((bf16[256,2048]{1,0:T(8,128)(2,1)S(1)}, bf16[256,2048]{1,0:T(8,128)(2,1)}, u32[]{:S(2)}) %copy-start.1) | copy-done | bytes 1048600
  3.8 0.0 copy-start.2
  3.8 1.1 %copy-done.2 = bf16[192,2048]{1,0:T(8,128)(2,1)S(1)} copy-done((bf16[192,2048]{1,0:T(8,128)(2,1)S(1)}, bf16[192,2048]{1,0:T(8,128)(2,1)}, u32[]{:S(2)}) %copy-start.2) | copy-done | bytes 786456
  4.9 0.0 copy-start.3
  4.9 0.9 %copy-done.3 = bf16[2048,64]{0,1:T(8,128)(2,1)S(1)} copy-done((bf16[2048,64]{0,1:T(8,128)(2,1)S(1)}, bf16[2048,64]{0,1:T(8,128)(2,1)}, u32[]{:S(2)}) %copy-start.3) | copy-done | bytes 262168
  5.8 0.0 copy-start.4
  5.8 0.9 %copy-done.4 = bf16[2048,64]{0,1:T(8,128)(2,1)S(1)} copy-done((bf16[2048,64]{0,1:T(8,128)(2,1)S(1)}, bf16[2048,64]{0,1:T(8,128)(2,1)}, u32[]{:S(2)}) %copy-start.4) | copy-done | bytes 262168
  6.8 23.5 %layer.1 = (bf16[48,2048]{1,0:T(8,128)(2,1)S(1)}, f32[4,192]{1,0:T(4,128)S(1)}) custom-call(bf16[192,2048]{1,0:T(8,128)(2,1)S(1)} %copy-done.2, bf16[2048,256]{1,0:T(8,128)(2,1)S(1)} %copy-done, bf16[64,2048]{1,0:T(8,128)(2,1)S(1)} %bitcast.4, bf16[64,2048]{1,0:T(8,128)(2,1)S(1)} %bitcast.5, bf16[256,2048]{1,0:T(8,128)(2,1)S(1)} %copy-done.1, ...), custom_call_target="tpu_custom_call" | custom-call | tf_op jit(solution)/shard_map/layer/pallas_call | solution.py:280
  30.3 0.7 %copy.11 = bf16[48,2048]{1,0:T(8,128)(2,1)} copy(bf16[48,2048]{1,0:T(8,128)(2,1)S(1)} %get-tuple-element.4) | data formatting | bytes 393216
  31.0 0.6 %copy.12 = f32[4,192]{1,0:T(4,128)} copy(f32[4,192]{1,0:T(4,128)S(1)} %get-tuple-element.5) | data formatting | bytes 6144
Async XLA Ops:
  0.6 0.7 %copy-start.5 = (f32[64]{0:T(128)S(1)}, f32[64]{0:T(128)}, u32[]{:S(2)}) copy-start(f32[64]{0:T(128)} %param.12) | copy-start | bytes 772
  0.6 0.7 %copy-start.6 = (f32[64]{0:T(128)S(1)}, f32[64]{0:T(128)}, u32[]{:S(2)}) copy-start(f32[64]{0:T(128)} %param.13) | copy-start | bytes 772
  1.3 1.2 %copy-start = (bf16[2048,256]{1,0:T(8,128)(2,1)S(1)}, bf16[2048,256]{1,0:T(8,128)(2,1)}, u32[]{:S(2)}) copy-start(bf16[2048,256]{1,0:T(8,128)(2,1)} %wq_hbm.1) | copy-start | bytes 3145732
  2.5 1.2 %copy-start.1 = (bf16[256,2048]{1,0:T(8,128)(2,1)S(1)}, bf16[256,2048]{1,0:T(8,128)(2,1)}, u32[]{:S(2)}) copy-start(bf16[256,2048]{1,0:T(8,128)(2,1)} %wo_hbm.1) | copy-start | bytes 3145732
  3.8 1.1 %copy-start.2 = (bf16[192,2048]{1,0:T(8,128)(2,1)S(1)}, bf16[192,2048]{1,0:T(8,128)(2,1)}, u32[]{:S(2)}) copy-start(bf16[192,2048]{1,0:T(8,128)(2,1)} %tok_hbm.1) | copy-start | bytes 2359300
  4.9 0.9 %copy-start.3 = (bf16[2048,64]{0,1:T(8,128)(2,1)S(1)}, bf16[2048,64]{0,1:T(8,128)(2,1)}, u32[]{:S(2)}) copy-start(bf16[2048,64]{0,1:T(8,128)(2,1)} %param.9) | copy-start | bytes 786436
  5.8 0.9 %copy-start.4 = (bf16[2048,64]{0,1:T(8,128)(2,1)S(1)}, bf16[2048,64]{0,1:T(8,128)(2,1)}, u32[]{:S(2)}) copy-start(bf16[2048,64]{0,1:T(8,128)(2,1)} %param.10) | copy-start | bytes 786436

commit v3 on v2

--- a/solution.py
+++ b/solution.py
@@ -274,7 +274,7 @@
         part = rows // n_tp
         chunk = width // CHUNKS
         n_out = n_sp // 2
-        hbm = pl.BlockSpec(memory_space=pltpu.HBM)
+        hbm = pl.BlockSpec(memory_space=pl.ANY)
         vmem = pl.BlockSpec(memory_space=pltpu.VMEM)
         dma = pltpu.SemaphoreType.DMA
         return pl.pallas_call(
@@ -308,7 +308,7 @@
                 dma((CHUNKS,)),
                 dma((CHUNKS,)),
             ],
-            compiler_params=pltpu.CompilerParams(collective_id=0, has_side_effects=True, vmem_limit_bytes=24 * 2**20),
+            compiler_params=pltpu.CompilerParams(collective_id=0, has_side_effects=True),
             name="layer",
         )(tokens, w_query, w_key.T, w_value.T, w_output, query_gain[None, :], key_gain[None, :])
 

time: 31.9 us -> 28.3 us (0.89)
  local copies, waits for them, and re-layouts: 7.41 us -> 2.21 us
  Pallas kernels: 23.5 us -> 25.3 us
    unnamed x16 -> x4, local copies, waits for them, and re-layouts: 7.41 us -> 2.21 us
    pallas_call x1, Pallas kernels: 23.5 us -> 25.3 us  [shards(): pl.pallas_call(functools.partial(kernel, n_sp, n_tp), out_shape=(jax.Shap...]
where the time goes in v3:
time: 28.3 us; the launch traced here: 28.2 us
  Pallas kernels  25.3 us (89%)
  local copies, waits for them, and re-layouts  2.21 us (8%)
  between operations  0.65 us (2%)
    pallas_call x1, Pallas kernels, shards(): pl.pallas_call(functools.partial(kernel, n_sp, n_tp), out_shape=(jax.Shap...  25.3 us
    unnamed x4, local copies, waits for them, and re-layouts  2.21 us

profile of v3, /device:TPU:0, one launch (start us, length us, event | category | flops | bytes accessed | tf_op | source)
XLA Modules:
  0.0 28.2 jit_solution(1299311590160956329)
XLA Ops:
  0.6 25.3 %layer.1 = (bf16[48,2048]{1,0:T(8,128)(2,1)}, f32[4,192]{1,0:T(4,128)}) custom-call(bf16[192,2048]{1,0:T(8,128)(2,1)} %tok_hbm.1, bf16[2048,256]{1,0:T(8,128)(2,1)} %wq_hbm.1, bf16[64,2048]{1,0:T(8,128)(2,1)} %bitcast.4, bf16[64,2048]{1,0:T(8,128)(2,1)} %bitcast.5, bf16[256,2048]{1,0:T(8,128)(2,1)} %wo_hbm.1, f32[1,64]{1,0:T(1,128)} %bitcast.6, f32[1,64]{1,0:T(1,128)} %bitcast.7), custom_call_target="tpu_custom_call" | custom-call | tf_op jit(solution)/shard_map/layer/pallas_call | solution.py:280
  26.0 0.0 copy-start
  26.0 1.6 %copy.11 = bf16[48,2048]{1,0:T(8,128)(2,1)} copy(bf16[48,2048]{1,0:T(8,128)(2,1)} %get-tuple-element.4) | data formatting | bytes 393216
  27.6 0.0 copy-done
  27.6 0.6 %copy.12 = f32[4,192]{1,0:T(4,128)} copy(f32[4,192]{1,0:T(4,128)S(1)} %copy-done) | data formatting | bytes 6144
Async XLA Ops:
  26.0 1.6 %copy-start = (f32[4,192]{1,0:T(4,128)S(1)}, f32[4,192]{1,0:T(4,128)}, u32[]{:S(2)}) copy-start(f32[4,192]{1,0:T(4,128)} %get-tuple-element.5) | copy-start | bytes 9220

commit v4 on v3

--- a/solution.py
+++ b/solution.py
@@ -54,9 +54,9 @@
 
 def kernel(
     n_sp, n_tp,
-    tok_hbm, wq_hbm, wk_hbm, wv_hbm, wo_hbm, qg_ref, kg_ref,
+    tok_hbm, wq_hbm, wk_hbm, wv_hbm, wo_hbm, qg_hbm, kg_hbm,
     out_ref, lse_ref,
-    tok, wq, w_kv, wo, kv_own, kvbuf, qpad, att, send_a, recv_a, keep, send_b, recv_b,
+    tok, wq, w_kv, wo, qg_ref, kg_ref, kv_own, kvbuf, qpad, att, send_a, recv_a, keep, send_b, recv_b,
     load_sem, send_sem, fwd_sem, recv_sem, a_send, a_recv, b_send, b_recv,
 ):
     rows = tok.shape[0]
@@ -88,10 +88,11 @@
             [
                 (tok_hbm, tok), (wv_hbm, w_kv.at[:head]), (wk_hbm, w_kv.at[head:]),
                 (wq_hbm, wq), (wo_hbm, wo),
+                (qg_hbm, qg_ref), (kg_hbm, kg_ref),
             ]
         )
     ]
-    for load in loads[:4]:
+    for load in loads[5:] + loads[:3]:
         load.start()
 
     barrier = pltpu.get_barrier_semaphore()
@@ -107,12 +108,15 @@
 
     tabs = tables(me * rows, rows, heads, head // 4)
     key_tabs = tuple(x[:, :rows] for x in tabs)
+    loads[5].wait()
+    loads[6].wait()
     gain_q = column(qg_ref[...]) * (head ** -0.5)
     gain_k = column(kg_ref[...])
 
     loads[0].wait()
     loads[1].wait()
     loads[2].wait()
+    loads[3].start()
     loads[4].start()
     raw_t = lax.dot_general(
         w_kv[...], tok[...], (((1,), (1,)), ((), ())), preferred_element_type=F32
@@ -142,12 +146,18 @@
             device_id={"sp": partner}, device_id_type=MESH,
         )
 
-    def arrival(i):
+    def land(i):
         pltpu.make_async_remote_copy(
             src_ref=slot(i), dst_ref=slot(i), send_sem=send_sem.at[0], recv_sem=recv_sem.at[i],
             device_id={"sp": partner}, device_id_type=MESH,
         ).wait_recv()
+
+    def held(i):
         return kvbuf[pl.ds(pl.multiple_of(i * rows, 16), rows), :]
+
+    def arrival(i):
+        land(i)
+        return held(i)
 
     pl.semaphore_wait(barrier, n_out + 2)
 
@@ -181,7 +191,6 @@
         return top, total, summed
 
     state = attend(kv_own[...], None)
-    state = attend(arrival(partner), state)
 
     def take_direct(d, state):
         i = origin(d) * 2 + minor
@@ -193,11 +202,20 @@
         return attend(arrival(origin(d) * 2 + 1 - minor), state)
 
     if n_out <= 8:
+        ready = partner
         for d in range(1, n_out):
-            state = take_direct(d, state)
+            i = origin(d) * 2 + minor
+            land(i)
+            forward(d).start()
+            if d == 1:
+                land(partner)
+            state = attend(held(ready), state)
+            ready = i
+        state = attend(held(ready), state)
         for d in range(1, n_out):
             state = take_forwarded(d, state)
     else:
+        state = attend(arrival(partner), state)
         state = lax.fori_loop(1, n_out, take_direct, state)
         state = lax.fori_loop(1, n_out, take_forwarded, state)
     top, total, summed = state
@@ -277,19 +295,24 @@
         hbm = pl.BlockSpec(memory_space=pl.ANY)
         vmem = pl.BlockSpec(memory_space=pltpu.VMEM)
         dma = pltpu.SemaphoreType.DMA
+        def stay(x):
+            return pltpu.with_memory_space_constraint(x, pltpu.HBM)
+
         return pl.pallas_call(
             functools.partial(kernel, n_sp, n_tp),
             out_shape=(
                 jax.ShapeDtypeStruct((part, width), BF16),
                 jax.ShapeDtypeStruct((heads, rows), F32),
             ),
-            in_specs=[hbm] * 5 + [vmem] * 2,
+            in_specs=[hbm] * 7,
             out_specs=(vmem, vmem),
             scratch_shapes=[
                 pltpu.VMEM((rows, depth), BF16),
                 pltpu.VMEM((depth, n_query), BF16),
                 pltpu.VMEM((2 * n_key, depth), BF16),
                 pltpu.VMEM((n_query, width), BF16),
+                pltpu.VMEM((1, head), F32),
+                pltpu.VMEM((1, head), F32),
                 pltpu.VMEM((rows, 2 * head), BF16),
                 pltpu.VMEM((n_sp * rows, 2 * head), BF16),
                 pltpu.VMEM((2 * head, heads * rows), BF16),
@@ -299,7 +322,7 @@
                 pltpu.VMEM((CHUNKS, part, chunk), F32),
                 pltpu.VMEM((CHUNKS, part, chunk), BF16),
                 pltpu.VMEM((CHUNKS, part, chunk), BF16),
-                dma((5,)),
+                dma((7,)),
                 dma((n_out,)),
                 dma((n_out,)),
                 dma((n_sp,)),
@@ -308,9 +331,12 @@
                 dma((CHUNKS,)),
                 dma((CHUNKS,)),
             ],
-            compiler_params=pltpu.CompilerParams(collective_id=0, has_side_effects=True),
+            compiler_params=pltpu.CompilerParams(collective_id=0, has_side_effects=True, vmem_limit_bytes=32 * 2**20),
             name="layer",
-        )(tokens, w_query, w_key.T, w_value.T, w_output, query_gain[None, :], key_gain[None, :])
+        )(
+            stay(tokens), stay(w_query), stay(w_key.T), stay(w_value.T), stay(w_output),
+            stay(query_gain[None, :]), stay(key_gain[None, :]),
+        )
 
     placed = (P("sp", None), P(None, "tp"), P(None, "tp"), P(None, "tp"), P("tp", None), P(), P())
     return jax.shard_map(

time: 28.3 us -> 25.8 us (0.912)
  Pallas kernels: 25.3 us -> 23.7 us
  local copies, waits for them, and re-layouts: 2.21 us -> 1.27 us
    pallas_call x1, Pallas kernels: 25.3 us -> 23.7 us  [shards(): pl.pallas_call(functools.partial(kernel, n_sp, n_tp), out_shape=(jax.Shap...]
    unnamed x4 -> x2, local copies, waits for them, and re-layouts: 2.21 us -> 1.27 us
where the time goes in v4:
time: 25.8 us; the launch traced here: 25.6 us
  Pallas kernels  23.7 us (92%)
  local copies, waits for them, and re-layouts  1.27 us (5%)
  between operations  0.64 us (2%)
    pallas_call x1, Pallas kernels, shards(): pl.pallas_call(functools.partial(kernel, n_sp, n_tp), out_shape=(jax.Shap...  23.7 us
    unnamed x2, local copies, waits for them, and re-layouts  1.27 us

profile of v4, /device:TPU:0, one launch (start us, length us, event | category | flops | bytes accessed | tf_op | source)
XLA Modules:
  0.0 25.6 jit_solution(17262635163949861881)
XLA Ops:
  0.6 23.7 %layer.1 = (bf16[48,2048]{1,0:T(8,128)(2,1)S(1)}, f32[4,192]{1,0:T(4,128)S(1)}) custom-call(bf16[192,2048]{1,0:T(8,128)(2,1)} %tok_hbm.1, bf16[2048,256]{1,0:T(8,128)(2,1)} %wq_hbm.1, bf16[64,2048]{1,0:T(8,128)(2,1)} %bitcast.4, bf16[64,2048]{1,0:T(8,128)(2,1)} %bitcast.5, bf16[256,2048]{1,0:T(8,128)(2,1)} %wo_hbm.1, f32[1,64]{1,0:T(1,128)} %bitcast.6, ...), custom_call_target="tpu_custom_call" | custom-call | tf_op jit(solution)/shard_map/layer/pallas_call | solution.py:301
  24.3 0.7 %copy.11 = bf16[48,2048]{1,0:T(8,128)(2,1)} copy(bf16[48,2048]{1,0:T(8,128)(2,1)S(1)} %get-tuple-element.4) | data formatting | bytes 393216
  25.0 0.6 %copy.12 = f32[4,192]{1,0:T(4,128)} copy(f32[4,192]{1,0:T(4,128)S(1)} %get-tuple-element.5) | data formatting | bytes 6144

commit v5 on v4

--- a/solution.py
+++ b/solution.py
@@ -124,33 +124,45 @@
     keys_t = prepare(raw_t[head:], gain_k, key_tabs)
     kv_own[...] = jnp.concatenate([raw_t[:head], keys_t], axis=0).T.astype(BF16)
 
-    def slot(i):
-        return kvbuf.at[pl.ds(pl.multiple_of(i * rows, 16), rows), :]
-
-    def to_partner():
-        return pltpu.make_async_remote_copy(
-            src_ref=kv_own, dst_ref=slot(me), send_sem=send_sem.at[0], recv_sem=recv_sem.at[me],
+    piece = rows // 2
+
+    def slot(i, k):
+        return kvbuf.at[pl.ds(pl.multiple_of(i * rows + k * piece, 16), piece), :]
+
+    def own(k):
+        return kv_own.at[pl.ds(k * piece, piece), :]
+
+    def to_partner(k):
+        return pltpu.make_async_remote_copy(
+            src_ref=own(k), dst_ref=slot(me, k), send_sem=send_sem.at[k], recv_sem=recv_sem.at[2 * me + k],
             device_id={"sp": partner}, device_id_type=MESH,
         )
 
-    def to_peer(d):
-        return pltpu.make_async_remote_copy(
-            src_ref=kv_own, dst_ref=slot(me), send_sem=send_sem.at[d], recv_sem=recv_sem.at[me],
+    def to_peer(d, k):
+        return pltpu.make_async_remote_copy(
+            src_ref=own(k), dst_ref=slot(me, k), send_sem=send_sem.at[2 * d + k],
+            recv_sem=recv_sem.at[2 * me + k],
             device_id={"sp": peer(d)}, device_id_type=MESH,
         )
 
-    def forward(d):
+    def forward(d, k):
         i = origin(d) * 2 + minor
         return pltpu.make_async_remote_copy(
-            src_ref=slot(i), dst_ref=slot(i), send_sem=fwd_sem.at[d], recv_sem=recv_sem.at[i],
+            src_ref=slot(i, k), dst_ref=slot(i, k), send_sem=fwd_sem.at[2 * d + k],
+            recv_sem=recv_sem.at[2 * i + k],
             device_id={"sp": partner}, device_id_type=MESH,
         )
 
-    def land(i):
+    def land_piece(i, k):
         pltpu.make_async_remote_copy(
-            src_ref=slot(i), dst_ref=slot(i), send_sem=send_sem.at[0], recv_sem=recv_sem.at[i],
+            src_ref=slot(i, k), dst_ref=slot(i, k), send_sem=send_sem.at[k],
+            recv_sem=recv_sem.at[2 * i + k],
             device_id={"sp": partner}, device_id_type=MESH,
         ).wait_recv()
+
+    def land(i):
+        land_piece(i, 0)
+        land_piece(i, 1)
 
     def held(i):
         return kvbuf[pl.ds(pl.multiple_of(i * rows, 16), rows), :]
@@ -162,11 +174,13 @@
     pl.semaphore_wait(barrier, n_out + 2)
 
     def send_peer(d, unused):
-        to_peer(d).start()
+        to_peer(d, 0).start()
+        to_peer(d, 1).start()
         return unused
 
     lax.fori_loop(1, n_out, send_peer, 0)
-    to_partner().start()
+    to_partner(0).start()
+    to_partner(1).start()
 
     loads[3].wait()
     raw_q = jnp.dot(tok[...], wq[...], preferred_element_type=F32).astype(BF16).astype(F32)
@@ -194,9 +208,10 @@
 
     def take_direct(d, state):
         i = origin(d) * 2 + minor
-        block = arrival(i)
-        forward(d).start()
-        return attend(block, state)
+        for k in range(2):
+            land_piece(i, k)
+            forward(d, k).start()
+        return attend(held(i), state)
 
     def take_forwarded(d, state):
         return attend(arrival(origin(d) * 2 + 1 - minor), state)
@@ -205,8 +220,9 @@
         ready = partner
         for d in range(1, n_out):
             i = origin(d) * 2 + minor
-            land(i)
-            forward(d).start()
+            for k in range(2):
+                land_piece(i, k)
+                forward(d, k).start()
             if d == 1:
                 land(partner)
             state = attend(held(ready), state)
@@ -269,12 +285,14 @@
         out_ref[:, cols] = (keep[c] + recv_b[c].astype(F32)).astype(BF16)
 
     def drain(d, unused):
-        to_peer(d).wait_send()
-        forward(d).wait_send()
+        for k in range(2):
+            to_peer(d, k).wait_send()
+            forward(d, k).wait_send()
         return unused
 
     lax.fori_loop(1, n_out, drain, 0)
-    to_partner().wait_send()
+    to_partner(0).wait_send()
+    to_partner(1).wait_send()
     for c in range(CHUNKS):
         copy_a(c).wait_send()
         copy_b(c).wait_send()
@@ -323,9 +341,9 @@
                 pltpu.VMEM((CHUNKS, part, chunk), BF16),
                 pltpu.VMEM((CHUNKS, part, chunk), BF16),
                 dma((7,)),
-                dma((n_out,)),
-                dma((n_out,)),
-                dma((n_sp,)),
+                dma((2 * n_out,)),
+                dma((2 * n_out,)),
+                dma((2 * n_sp,)),
                 dma((CHUNKS,)),
                 dma((CHUNKS,)),
                 dma((CHUNKS,)),

time: 25.8 us -> 25.9 us (level)
  no operation moved by 1% of the time
where the time goes in v5:
time: 25.9 us; the launch traced here: 25.7 us
  Pallas kernels  23.8 us (92%)
  local copies, waits for them, and re-layouts  1.27 us (5%)
  between operations  0.64 us (2%)
    pallas_call x1, Pallas kernels, shards(): pl.pallas_call(functools.partial(kernel, n_sp, n_tp), out_shape=(jax.Shap...  23.8 us
    unnamed x2, local copies, waits for them, and re-layouts  1.27 us

profile of v5, /device:TPU:0, one launch (start us, length us, event | category | flops | bytes accessed | tf_op | source)
XLA Modules:
  0.0 25.7 jit_solution(10526399463364755208)
XLA Ops:
  0.6 23.8 %layer.1 = (bf16[48,2048]{1,0:T(8,128)(2,1)S(1)}, f32[4,192]{1,0:T(4,128)S(1)}) custom-call(bf16[192,2048]{1,0:T(8,128)(2,1)} %tok_hbm.1, bf16[2048,256]{1,0:T(8,128)(2,1)} %wq_hbm.1, bf16[64,2048]{1,0:T(8,128)(2,1)} %bitcast.4, bf16[64,2048]{1,0:T(8,128)(2,1)} %bitcast.5, bf16[256,2048]{1,0:T(8,128)(2,1)} %wo_hbm.1, f32[1,64]{1,0:T(1,128)} %bitcast.6, ...), custom_call_target="tpu_custom_call" | custom-call | tf_op jit(solution)/shard_map/layer/pallas_call | solution.py:319
  24.4 0.7 %copy.11 = bf16[48,2048]{1,0:T(8,128)(2,1)} copy(bf16[48,2048]{1,0:T(8,128)(2,1)S(1)} %get-tuple-element.4) | data formatting | bytes 393216
  25.1 0.6 %copy.12 = f32[4,192]{1,0:T(4,128)} copy(f32[4,192]{1,0:T(4,128)S(1)} %get-tuple-element.5) | data formatting | bytes 6144
